TPU v7x, 32 devices: a whole 2x2x4 slice. The times are simulated.
32 devices in a mesh: gr: 2 (over core), sp: 8 (over z, y), tp: 2 (over x).
Axes of the slice: x: 2, y: 2, z: 4, core: 2. Of those that a mesh axis runs over, the one named last changes fastest.
Arguments:
- tokens: bfloat16 [4, 2048, 2048], P('gr', ('sp', 'tp')), parts along dimension 0, may hold values from -6 to 6
- key_weight: bfloat16 [2048, 1024], P('sp'), may hold values from -0.125 to 0.125
- value_weight: bfloat16 [2048, 1024], P('sp'), may hold values from -0.125 to 0.125
- queries: bfloat16 [4, 1024], P('gr'), parts along dimension 0, may hold values from -6 to 6
- head_offset: float32 [16], replicated, may hold values from -14 to -3.5
- key_bias: bfloat16 [4, 2048, 16], P('gr', ('sp', 'tp')), parts along dimension 0, may hold values from -0.5 to 12.9
Outputs:
- key_cache: bfloat16 [4, 2048, 1024], P('gr', 'sp', 'tp'), parts along dimension 0
- value_cache: bfloat16 [4, 2048, 1024], P('gr', 'sp', 'tp'), parts along dimension 0
- bias_cache: bfloat16 [4, 2048, 16], P('gr', 'sp', 'tp'), parts along dimension 0
- reading: float32 [4, 1024], P('gr', 'tp'), parts along dimension 0
There are 2 independent parts, one for each index of `gr`. A program takes and returns all parts, laid end to end along the dimension named above; an argument that names none is the same for every part. Nothing has to cross between parts.
All inputs are finite; a program needn't handle non-finite values.
Results may differ from a plain program's by a relative error of at most 0.0052.
Values may be sent and summed in bfloat16 or wider, within the bound.
A program may use at most 64 MiB of HBM per device.

v0:
```python
import jax
import jax.numpy as jnp
from jax import lax
from jax.sharding import PartitionSpec as P


def carried_in(x, axis, combine, identity):
    length, position = (lax.axis_size(axis), lax.axis_index(axis))
    everything = lax.all_gather(x, axis)
    start = jnp.broadcast_to(jnp.asarray(identity, x.dtype), x.shape)

    def lap(k, before):
        at = length - 1 - k
        reached = at > position
        new = combine(before, everything[at])
        return jnp.where(reached, new, before)

    return lax.fori_loop(0, length, lap, start)


def add_terms(earlier, later):
    return earlier + later


def normalize(mixture):
    return mixture * lax.rsqrt(jnp.mean(mixture * mixture, axis=-1, keepdims=True) + 1e-06)


def per_device(tokens, key_weight, value_weight, queries, head_offset, key_bias):
    seq_count, pos_dev, model_width = tokens.shape
    head_count = head_offset.shape[0]
    kv_width = key_weight.shape[1]
    head_dim = kv_width // head_count
    score_scale = head_dim ** (-0.5)
    tp_count = lax.axis_size("tp")
    col_width = kv_width // tp_count
    col_start = lax.axis_index("tp") * col_width
    own_cols = jnp.concatenate(
        [
            lax.dynamic_slice_in_dim(key_weight, col_start, col_width, 1),
            lax.dynamic_slice_in_dim(value_weight, col_start, col_width, 1),
        ],
        axis=1,
    )
    full_cols = lax.all_gather(own_cols, "sp", axis=0, tiled=True)
    projected = jnp.einsum(
        "spd,dw->spw",
        lax.all_gather(tokens, "tp", axis=1, tiled=True),
        full_cols,
        preferred_element_type=jnp.float32,
    ).astype(jnp.bfloat16)
    key_cache = projected[:, :, :col_width]
    value_cache = projected[:, :, col_width:]
    bias_cache = lax.all_to_all(key_bias, "tp", split_axis=2, concat_axis=1, tiled=True)
    span_len = key_cache.shape[1]
    local_heads = bias_cache.shape[2]
    key_blocks = key_cache.reshape(seq_count, span_len, local_heads, head_dim)
    value_blocks = value_cache.reshape(seq_count, span_len, local_heads, head_dim)
    query_cols = lax.dynamic_slice_in_dim(queries, col_start, col_width, 1)
    query_heads = query_cols.reshape(seq_count, local_heads, head_dim)
    head_start = lax.axis_index("tp") * local_heads
    local_offset = lax.dynamic_slice_in_dim(head_offset, head_start, local_heads, 0)
    logits = (
        jnp.einsum("sphc,shc->shp", key_blocks, query_heads, preferred_element_type=jnp.float32)
        * score_scale
    )
    logits = (
        logits
        + local_offset[None, :, None]
        + jnp.transpose(bias_cache.astype(jnp.float32), (0, 2, 1))
    )
    fading = jax.nn.log_sigmoid(-logits)
    within = lax.cumsum(fading, axis=2, reverse=True) - fading
    block_total = jnp.sum(fading, axis=2)
    carried = carried_in(block_total, "sp", add_terms, jnp.zeros_like(block_total))
    weights = jnp.exp(jax.nn.log_sigmoid(logits) + within + carried[:, :, None]).astype(
        jnp.bfloat16
    )
    partial_value = jnp.einsum(
        "shp,sphc->shc", weights, value_blocks, preferred_element_type=jnp.float32
    )
    mixture = lax.psum(partial_value, "sp")
    reading = normalize(mixture).reshape(seq_count, col_width)
    return (key_cache, value_cache, bias_cache, reading)


def solution(mesh):
    in_specs = (
        P("gr", ("sp", "tp"), None),
        P("sp", None),
        P("sp", None),
        P("gr", None),
        P(),
        P("gr", ("sp", "tp"), None),
    )
    out_specs = (P("gr", "sp", "tp"), P("gr", "sp", "tp"), P("gr", "sp", "tp"), P("gr", "tp"))
    return jax.shard_map(
        per_device, mesh=mesh, in_specs=in_specs, out_specs=out_specs, check_vma=False
    )
```

profile of v0, /device:TPU:0, one launch (start us, length us, event | category | flops | bytes accessed | tf_op | source)
XLA Modules:
  0.0 179.6 jit_solution(294673093222609058)
XLA Ops:
  7.2 0.7 all-gather.7.cloned.1.call-update
  8.0 1.1 constant_dynamic-slice_fusion.1
  9.1 0.1 copy.28
  9.2 0.1 copy.29
  9.3 0.8 pad_maximum_fusion
  10.2 0.6 copy.20
  10.8 4.2 %all-to-all-start = ((bf16[2,128,16]{1,0,2:T(2,128)(2,1)}), bf16[2,128,16]{1,0,2:T(2,128)(2,1)S(1)}, u32[]{:S(2)}, u32[]{:S(2)}) async-start(bf16[2,128,16]{1,0,2:T(2,128)(2,1)} %copy.20), calls=%async_computation | async-start | bytes 16384 | tf_op jit(solution)/shard_map/all_to_all | solution.py:54
  15.2 30.2 %all-gather.7.cloned.1.call-done = bf16[2,256,2048]{2,1,0:T(8,128)(2,1)} async-done(((bf16[2,128,2048]{2,1,0:T(8,128)(2,1)}), bf16[2,256,2048]{2,1,0:T(8,128)(2,1)}) %all-gather.7.cloned.1.call-update) | async-done | bytes 2097168 | tf_op jit(solution)/shard_map/all_gather | solution.py:48
  45.4 77.3 %all-gather.5.cloned.1.call-done = bf16[2048,1024]{0,1:T(8,128)(2,1)} async-done(((bf16[256,1024]{0,1:T(8,128)(2,1)}), bf16[2048,1024]{0,1:T(8,128)(2,1)}) %all-gather.5.cloned.1.call-update) | async-done | bytes 4194320 | tf_op jit(solution)/shard_map/all_gather | solution.py:45
  122.7 5.2 %fusion.5 = bf16[2,256,1024]{1,2,0:T(8,128)(2,1)S(1)} fusion(bf16[2,256,2048]{2,1,0:T(8,128)(2,1)} %all-gather.7.cloned.1.call-done, bf16[2048,1024]{0,1:T(8,128)(2,1)} %all-gather.5.cloned.1.call-done), kind=kOutput, calls=%fused_computation.4 | convolution fusion | flops 2148007936 | bytes 7340032 | tf_op jit(solution)/shard_map/spd,dw->spw/dot_general | solution.py:46
  128.0 0.2 fusion.19
  128.2 1.0 copy.22
  129.2 0.1 negate_bitcast_fusion
  129.3 0.2 fusion.16
  129.5 17.7 %all-gather.1 = f32[8,2,8]{2,1,0:T(2,128)S(1)} all-gather(f32[1,2,8]{2,1,0:T(2,128)S(1)} %negate_bitcast_fusion.1), channel_id=2, replica_groups=mesh['gr'=2,'sp'=8,'tp'=2] {'sp'}, dimensions={0}, use_global_device_ids=true | all-gather | bytes 576 | tf_op jit(solution)/shard_map/all_gather | solution.py:9
  147.2 0.3 while.16
  147.5 5.0 %reduce-window.6 = f32[2,8,2,128]{3,1,2,0:T(8,128)S(1)} reduce-window(f32[2,8,2,128]{3,1,2,0:T(8,128)S(1)} %get-tuple-element.150, f32[]{:T(128)} %constant.72.clone.1), window={size=1x1x1x128 pad=0_0x0_0x0_0x0_127}, to_apply=%region_0.1 | reduce-window | flops 520192 | bytes 32772 | tf_op jit(solution)/shard_map/reduce-window
  152.5 0.1 slice_reduce_fusion
  152.6 1.0 copy.23
  153.6 0.1 fusion.17
  153.7 0.2 fusion.14
  153.9 17.9 %psum.7 = f32[2,8,64]{2,1,0:T(8,128)S(1)} all-reduce(f32[2,8,64]{2,1,0:T(8,128)S(1)} %bitcast.62), channel_id=1, replica_groups=mesh['gr'=2,'sp'=8,'tp'=2] {'sp'}, use_global_device_ids=true, to_apply=%region_5.6 | all-reduce | flops 1024 | bytes 8192 | tf_op jit(solution)/shard_map/psum | solution.py:82
  171.9 0.1 multiply_reduce_fusion
  172.1 0.7 reshape.53
  (30 shorter events, 0.6 us)
Async XLA Ops:
  7.2 7.9 %copy-start = (bf16[2,1024]{1,0:T(2,128)(2,1)S(1)}, bf16[2,1024]{1,0:T(2,128)(2,1)}, u32[]{:S(2)}) copy-start(bf16[2,1024]{1,0:T(2,128)(2,1)} %param.11) | copy-start | bytes 12292
  7.2 38.2 %all-gather.7.cloned.1.call-start = ((), (), s32[]{:S(2)}) async-start(), calls=%async_computation.2 | async-start | bytes 3145728 | tf_op jit(solution)/shard_map/all_gather | solution.py:48
  7.9 2.3 %copy-start.2 = (bf16[2,128,16]{1,2,0:T(8,128)(2,1)S(1)}, bf16[2,128,16]{1,2,0:T(8,128)(2,1)}, u32[]{:S(2)}) copy-start(bf16[2,128,16]{1,2,0:T(8,128)(2,1)} %param.13) | copy-start | bytes 24580
  7.9 7.2 %copy-start.3 = (f32[16]{0:T(128)S(1)}, f32[16]{0:T(128)}, u32[]{:S(2)}) copy-start(f32[16]{0:T(128)} %param.12) | copy-start | bytes 196
  7.9 114.7 %all-gather.5.cloned.1.call-start = ((), (), s32[]{:S(2)}) async-start(), calls=%async_computation.1 | async-start | bytes 4718592 | tf_op jit(solution)/shard_map/all_gather | solution.py:45
  10.8 118.4 %all-to-all-start = ((bf16[2,128,16]{1,0,2:T(2,128)(2,1)}), bf16[2,128,16]{1,0,2:T(2,128)(2,1)S(1)}, u32[]{:S(2)}, u32[]{:S(2)}) async-start(bf16[2,128,16]{1,0,2:T(2,128)(2,1)} %copy.20), calls=%async_computation | async-start | bytes 16384 | tf_op jit(solution)/shard_map/all_to_all | solution.py:54
  129.3 43.5 %copy-start.1 = (bf16[2,256,8]{1,2,0:T(8,128)(2,1)}, bf16[2,256,8]{1,2,0:T(8,128)(2,1)S(1)}, u32[]{:S(2)}) copy-start(bf16[2,256,8]{1,2,0:T(8,128)(2,1)S(1)} %get-tuple-element.151) | copy-start | bytes 24580
Sparse Core Ops, SparseCore 0:
  9.5 35.8 all-gather.6
  48.0 74.6 all-gather.4
where the time goes:
time: 180 us
  waiting for transfers between devices  108 us (60%)
  blocking collectives  35.7 us (20%)
  between operations  14.2 us (8%)
  other arithmetic  6.49 us (4%)
  matrix products  5.64 us (3%)
  local copies, waits for them, and re-layouts  4.99 us (3%)
  starting transfers between devices  4.31 us (2%)
    all_gather x1, waiting for transfers between devices, per_device(): full_cols = lax.all_gather(own_cols, 'sp', axis=0, tiled=True)  77.3 us
    all_gather x1, waiting for transfers between devices, per_device(): lax.all_gather(tokens, 'tp', axis=1, tiled=True)  30.2 us
    psum x1, blocking collectives, per_device(): mixture = lax.psum(partial_value, 'sp')  17.9 us
    all_gather x1, blocking collectives, carried_in(): everything = lax.all_gather(x, axis)  17.7 us
    dot_general x1, matrix products, per_device(): jnp.einsum('spd,dw->spw', lax.all_gather(tokens, 'tp', axis=1, tiled=True...  5.22 us
    another operation x2, other arithmetic  5.02 us
    all_to_all x1, starting transfers between devices, per_device(): lax.all_to_all(key_bias, 'tp', split_axis=2, concat_axis=1, tiled=True)  4.23 us
  transfers between devices with their start and end apart: 3, of which 2 were waited for; matrix products, arithmetic and copies ran while one was open for 5% of the time, Pallas kernels for 0%

commit v1 on v0

--- a/solution.py
+++ b/solution.py
@@ -1,7 +1,25 @@
+import functools
 import jax
 import jax.numpy as jnp
 from jax import lax
 from jax.sharding import PartitionSpec as P
+
+
+def cut_quotas_all(field_in, comm_axis):
+    fan = lax.axis_size(comm_axis)
+    local_next = field_in
+    for i0 in [t for t in (1, 2, 4, 8, 16) if t < fan]:
+        ledger = []
+        h = 0
+        while h < fan:
+            ledger.append((h, h ^ i0))
+            h += 1
+        opened = lax.ppermute(local_next, comm_axis, ledger)
+        local_next = local_next + opened
+    return local_next
+
+
+group_sample_on = functools.partial(cut_quotas_all, comm_axis="sp")
 
 
 def carried_in(x, axis, combine, identity):
@@ -79,7 +97,7 @@
     partial_value = jnp.einsum(
         "shp,sphc->shc", weights, value_blocks, preferred_element_type=jnp.float32
     )
-    mixture = lax.psum(partial_value, "sp")
+    mixture = group_sample_on(partial_value)
     reading = normalize(mixture).reshape(seq_count, col_width)
     return (key_cache, value_cache, bias_cache, reading)
 

time: 180 us -> 172 us (0.956)
  blocking collectives: 35.7 us -> 17.7 us
  waiting for transfers between devices: 108 us -> 117 us
    psum x1 -> x0, blocking collectives: 17.9 us -> none  [per_device(): mixture = lax.psum(partial_value, 'sp')]
    ppermute x0 -> x3, waiting for transfers between devices: none -> 9.26 us  [cut_quotas_all(): opened = lax.ppermute(local_next, comm_axis, ledger)]
  transfers between devices with their start and end apart: 3 -> 6, of which waited for: 2 -> 5; matrix products, arithmetic and copies ran while one was open for 5% -> 6% of each run, Pallas kernels for 0% -> 0%
where the time goes in v1:
time: 172 us
  waiting for transfers between devices  117 us (68%)
  blocking collectives  17.7 us (10%)
  between operations  14.2 us (8%)
  other arithmetic  6.51 us (4%)
  matrix products  5.64 us (3%)
  local copies, waits for them, and re-layouts  4.98 us (3%)
  starting transfers between devices  4.9 us (3%)
    all_gather x1, waiting for transfers between devices, per_device(): full_cols = lax.all_gather(own_cols, 'sp', axis=0, tiled=True)  77.3 us
    all_gather x1, waiting for transfers between devices, per_device(): lax.all_gather(tokens, 'tp', axis=1, tiled=True)  30.2 us
    all_gather x1, blocking collectives, carried_in(): everything = lax.all_gather(x, axis)  17.7 us
    ppermute x3, waiting for transfers between devices, cut_quotas_all(): opened = lax.ppermute(local_next, comm_axis, ledger)  9.26 us
    dot_general x1, matrix products, per_device(): jnp.einsum('spd,dw->spw', lax.all_gather(tokens, 'tp', axis=1, tiled=True...  5.23 us
    another operation x2, other arithmetic  5.02 us
    all_to_all x1, starting transfers between devices, per_device(): lax.all_to_all(key_bias, 'tp', split_axis=2, concat_axis=1, tiled=True)  4.23 us
  transfers between devices with their start and end apart: 6, of which 5 were waited for; matrix products, arithmetic and copies ran while one was open for 6% of the time, Pallas kernels for 0%

profile of v1, /device:TPU:0, one launch (start us, length us, event | category | flops | bytes accessed | tf_op | source)
XLA Modules:
  0.0 171.5 jit_solution(9571162010687550313)
XLA Ops:
  7.2 0.7 all-gather.7.cloned.1.call-update
  8.0 1.1 constant_dynamic-slice_fusion.1
  9.1 0.1 copy.28
  9.2 0.1 copy.29
  9.3 0.8 pad_maximum_fusion
  10.2 0.6 copy.20
  10.8 4.2 %all-to-all-start = ((bf16[2,128,16]{1,0,2:T(2,128)(2,1)}), bf16[2,128,16]{1,0,2:T(2,128)(2,1)S(1)}, u32[]{:S(2)}, u32[]{:S(2)}) async-start(bf16[2,128,16]{1,0,2:T(2,128)(2,1)} %copy.20), calls=%async_computation | async-start | bytes 16384 | tf_op jit(solution)/shard_map/all_to_all | solution.py:72
  15.2 30.2 %all-gather.7.cloned.1.call-done = bf16[2,256,2048]{2,1,0:T(8,128)(2,1)} async-done(((bf16[2,128,2048]{2,1,0:T(8,128)(2,1)}), bf16[2,256,2048]{2,1,0:T(8,128)(2,1)}) %all-gather.7.cloned.1.call-update) | async-done | bytes 2097168 | tf_op jit(solution)/shard_map/all_gather | solution.py:66
  45.4 77.3 %all-gather.5.cloned.1.call-done = bf16[2048,1024]{0,1:T(8,128)(2,1)} async-done(((bf16[256,1024]{0,1:T(8,128)(2,1)}), bf16[2048,1024]{0,1:T(8,128)(2,1)}) %all-gather.5.cloned.1.call-update) | async-done | bytes 4194320 | tf_op jit(solution)/shard_map/all_gather | solution.py:63
  122.7 5.2 %fusion.5 = bf16[2,256,1024]{1,2,0:T(8,128)(2,1)S(1)} fusion(bf16[2,256,2048]{2,1,0:T(8,128)(2,1)} %all-gather.7.cloned.1.call-done, bf16[2048,1024]{0,1:T(8,128)(2,1)} %all-gather.5.cloned.1.call-done), kind=kOutput, calls=%fused_computation.4 | convolution fusion | flops 2148007936 | bytes 7340032 | tf_op jit(solution)/shard_map/spd,dw->spw/dot_general | solution.py:64
  128.0 0.2 fusion.19
  128.3 0.2 fusion.16
  128.5 17.7 %all-gather.1 = f32[8,2,8]{2,1,0:T(2,128)S(1)} all-gather(f32[1,2,8]{2,1,0:T(2,128)S(1)} %negate_bitcast_fusion.1), channel_id=2, replica_groups=mesh['gr'=2,'sp'=8,'tp'=2] {'sp'}, dimensions={0}, use_global_device_ids=true | all-gather | bytes 576 | tf_op jit(solution)/shard_map/all_gather | solution.py:27
  146.2 0.3 while.16
  146.5 5.0 %reduce-window.6 = f32[2,8,2,128]{3,1,2,0:T(8,128)S(1)} reduce-window(f32[2,8,2,128]{3,1,2,0:T(8,128)S(1)} %get-tuple-element.152, f32[]{:T(128)} %constant.72.clone.1), window={size=1x1x1x128 pad=0_0x0_0x0_0x0_127}, to_apply=%region_0.1 | reduce-window | flops 520192 | bytes 32772 | tf_op jit(solution)/shard_map/reduce-window
  151.6 0.1 fusion.17
  151.7 0.2 fusion.14
  151.9 0.6 collective-permute-start
  152.5 3.1 %collective-permute-done = f32[2,8,64]{2,1,0:T(8,128)S(1)} collective-permute-done((f32[2,8,64]{2,1,0:T(8,128)S(1)}, f32[2,8,64]{2,1,0:T(8,128)S(1)}, u32[]{:S(2)}, u32[]{:S(2)}) %collective-permute-start) | collective-permute-done | bytes 4128 | tf_op jit(solution)/shard_map/ppermute | solution.py:17
  155.6 3.6 %collective-permute-done.1 = f32[2,8,64]{2,1,0:T(8,128)S(1)} collective-permute-done((f32[2,8,64]{2,1,0:T(8,128)S(1)}, f32[2,8,64]{2,1,0:T(8,128)S(1)}, u32[]{:S(2)}, u32[]{:S(2)}) %collective-permute-start.1) | collective-permute-done | bytes 4128 | tf_op jit(solution)/shard_map/ppermute | solution.py:17
  159.3 1.0 copy.22
  160.3 1.0 copy.23
  161.3 2.5 %collective-permute-done.2 = f32[2,8,64]{2,1,0:T(8,128)S(1)} collective-permute-done((f32[2,8,64]{2,1,0:T(8,128)S(1)}, f32[2,8,64]{2,1,0:T(8,128)S(1)}, u32[]{:S(2)}, u32[]{:S(2)}) %collective-permute-start.2) | collective-permute-done | bytes 4128 | tf_op jit(solution)/shard_map/ppermute | solution.py:17
  164.0 0.7 reshape.53
  (37 shorter events, 0.9 us)
Async XLA Ops:
  7.2 7.9 %copy-start = (bf16[2,1024]{1,0:T(2,128)(2,1)S(1)}, bf16[2,1024]{1,0:T(2,128)(2,1)}, u32[]{:S(2)}) copy-start(bf16[2,1024]{1,0:T(2,128)(2,1)} %param.11) | copy-start | bytes 12292
  7.2 38.2 %all-gather.7.cloned.1.call-start = ((), (), s32[]{:S(2)}) async-start(), calls=%async_computation.2 | async-start | bytes 3145728 | tf_op jit(solution)/shard_map/all_gather | solution.py:66
  7.9 2.3 %copy-start.2 = (bf16[2,128,16]{1,2,0:T(8,128)(2,1)S(1)}, bf16[2,128,16]{1,2,0:T(8,128)(2,1)}, u32[]{:S(2)}) copy-start(bf16[2,128,16]{1,2,0:T(8,128)(2,1)} %param.13) | copy-start | bytes 24580
  7.9 7.2 %copy-start.3 = (f32[16]{0:T(128)S(1)}, f32[16]{0:T(128)}, u32[]{:S(2)}) copy-start(f32[16]{0:T(128)} %param.12) | copy-start | bytes 196
  7.9 114.7 %all-gather.5.cloned.1.call-start = ((), (), s32[]{:S(2)}) async-start(), calls=%async_computation.1 | async-start | bytes 4718592 | tf_op jit(solution)/shard_map/all_gather | solution.py:63
  10.8 117.4 %all-to-all-start = ((bf16[2,128,16]{1,0,2:T(2,128)(2,1)}), bf16[2,128,16]{1,0,2:T(2,128)(2,1)S(1)}, u32[]{:S(2)}, u32[]{:S(2)}) async-start(bf16[2,128,16]{1,0,2:T(2,128)(2,1)} %copy.20), calls=%async_computation | async-start | bytes 16384 | tf_op jit(solution)/shard_map/all_to_all | solution.py:72
  128.3 36.4 %copy-start.1 = (bf16[2,256,8]{1,2,0:T(8,128)(2,1)}, bf16[2,256,8]{1,2,0:T(8,128)(2,1)S(1)}, u32[]{:S(2)}) copy-start(bf16[2,256,8]{1,2,0:T(8,128)(2,1)S(1)} %get-tuple-element.153) | copy-start | bytes 24580
  151.9 3.7 %collective-permute-start = (f32[2,8,64]{2,1,0:T(8,128)S(1)}, f32[2,8,64]{2,1,0:T(8,128)S(1)}, u32[]{:S(2)}, u32[]{:S(2)}) collective-permute-start(f32[2,8,64]{2,1,0:T(8,128)S(1)} %bitcast.62), channel_id=1, source_target_pairs={{0,2},{2,0},{4,6},{6,4},{8,10},{10,8},{12,14},{14,12},{1,3},{3,1},... | collective-permute-start | bytes 12296 | tf_op jit(solution)/shard_map/ppermute | solution.py:17
  155.6 3.7 %collective-permute-start.1 = (f32[2,8,64]{2,1,0:T(8,128)S(1)}, f32[2,8,64]{2,1,0:T(8,128)S(1)}, u32[]{:S(2)}, u32[]{:S(2)}) collective-permute-start(f32[2,8,64]{2,1,0:T(8,128)S(1)} %add.105), channel_id=1, source_target_pairs={{0,4},{2,6},{4,0},{6,2},{8,12},{10,14},{12,8},{14,10},{1,5},{3,7},... | collective-permute-start | bytes 12296 | tf_op jit(solution)/shard_map/ppermute | solution.py:17
  159.3 4.5 %collective-permute-start.2 = (f32[2,8,64]{2,1,0:T(8,128)S(1)}, f32[2,8,64]{2,1,0:T(8,128)S(1)}, u32[]{:S(2)}, u32[]{:S(2)}) collective-permute-start(f32[2,8,64]{2,1,0:T(8,128)S(1)} %add.106), channel_id=1, source_target_pairs={{0,8},{2,10},{4,12},{6,14},{8,0},{10,2},{12,4},{14,6},{1,9},{3,11}... | collective-permute-start | bytes 12296 | tf_op jit(solution)/shard_map/ppermute | solution.py:17
Sparse Core Ops, SparseCore 0:
  9.5 35.8 all-gather.6
  48.0 74.6 all-gather.4
